TPU v7x, 32 devices: a whole 2x2x4 slice. The times are simulated.
32 devices in a mesh: dp: 2 (over x), kv: 8 (over z, y), tp: 2 (over core).
Axes of the slice: x: 2, y: 2, z: 4, core: 2. Of those that a mesh axis runs over, the one named last changes fastest.
Arguments:
- tokens: bfloat16 [2, 1536, 2048], P('dp', 'kv'), may hold values from -60 to 60
- doc_lengths: int32 [2, 8], P('dp'), may hold values from 1 to 768, as said below
- picked: int32 [2, 48, 32], P('dp', 'kv'), may hold values from -1 to 47, as said below
- w_query: bfloat16 [2048, 1024], P(None, 'tp'), may hold values from -0.125 to 0.125
- w_key: bfloat16 [2048, 128], replicated, may hold values from -0.125 to 0.125
- w_value: bfloat16 [2048, 128], replicated, may hold values from -0.125 to 0.125
- w_out: bfloat16 [1024, 2048], replicated, may hold values from -0.1875 to 0.1875
Outputs:
- mixed: bfloat16 [2, 1536, 2048], P('dp', 'kv')
Inputs may be any that keep to these rules, and one draw needn't show every extreme that they name: `doc_lengths`: each row sums to 1536; its largest document has exactly 768 positions. `picked`: slot 0 of query block b is b itself; the other slots hold distinct blocks before b, or -1 when fewer such blocks are named. Of the 6 blocks that one device of kv holds, at most 2 are named by query blocks held by other devices of kv, and in every row some device reaches 2.
All inputs are finite; a program needn't handle non-finite values.
Results may differ from a plain program's by a relative error of at most 0.011.
Values may be sent and summed in bfloat16 or wider, within the bound.
A program may use at most 64 MiB of HBM per device.

v0:
```python
import jax
import jax.numpy as jnp
from jax import lax
from jax.sharding import PartitionSpec as P

KV_HEADS = 2
HEAD_DIM = 64
BLOCK = 32
PICKS = 32


def rotate(values_in, positions):
    half = values_in.shape[-1] // 2
    inverse = 10000.0 ** (-jnp.arange(half, dtype=jnp.float32) / half)
    angles = positions.astype(jnp.float32)[:, None] * inverse[None, :]
    cosine = jnp.cos(angles)[:, None, :]
    sine = jnp.sin(angles)[:, None, :]
    first = values_in[..., :half]
    second = values_in[..., half:]
    return jnp.concatenate(
        [first * cosine - second * sine, second * cosine + first * sine], axis=-1
    )


def doc_of(positions, ends):
    return jnp.sum((positions[..., None] >= ends).astype(jnp.int32), axis=-1)


def shards(tokens, doc_lengths, picked, w_query, w_key, w_value, w_out):
    local = tokens[0]
    rows = local.shape[0]
    kv_index = lax.axis_index("kv")
    tp_index = lax.axis_index("tp")
    positions = kv_index * rows + jnp.arange(rows, dtype=jnp.int32)
    heads_dev = w_query.shape[1] // HEAD_DIM
    kv_dev = KV_HEADS // lax.axis_size("tp")
    group = heads_dev // kv_dev
    width = kv_dev * HEAD_DIM
    queries = rotate(
        jnp.dot(local, w_query, preferred_element_type=jnp.float32).reshape(
            rows, heads_dev, HEAD_DIM
        ),
        positions,
    ).astype(jnp.bfloat16)
    key_cols = lax.dynamic_slice_in_dim(w_key, tp_index * width, width, 1)
    value_cols = lax.dynamic_slice_in_dim(w_value, tp_index * width, width, 1)
    keys = rotate(
        jnp.dot(local, key_cols, preferred_element_type=jnp.float32).reshape(
            rows, kv_dev, HEAD_DIM
        ),
        positions,
    ).astype(jnp.bfloat16)
    values = jnp.dot(local, value_cols, preferred_element_type=jnp.float32).astype(jnp.bfloat16)
    packed = jnp.concatenate([keys.reshape(rows, width), values], axis=1)
    ends = jnp.cumsum(doc_lengths[0])
    blocks_dev = rows // BLOCK
    slots = picked[0]
    offsets = jnp.arange(BLOCK, dtype=jnp.int32)
    chosen = jnp.maximum(slots, 0)
    key_pos = (chosen[:, :, None] * BLOCK + offsets[None, None, :]).reshape(
        blocks_dev, PICKS * BLOCK
    )
    every = lax.all_gather(packed, "kv", axis=0, tiled=True)
    selected = every[key_pos]
    block_keys = selected[..., :width].reshape(blocks_dev, PICKS * BLOCK, kv_dev, HEAD_DIM)
    block_values = selected[..., width:].reshape(blocks_dev, PICKS * BLOCK, kv_dev, HEAD_DIM)
    query_pos = positions.reshape(blocks_dev, BLOCK)
    filled = jnp.repeat(slots >= 0, BLOCK, axis=1)
    live = (
        filled[:, None, :]
        & (key_pos[:, None, :] <= query_pos[:, :, None])
        & (doc_of(key_pos, ends)[:, None, :] == doc_of(query_pos, ends)[:, :, None])
    )
    grouped = queries.reshape(blocks_dev, BLOCK, kv_dev, group, HEAD_DIM)
    scores = jnp.einsum(
        "bqngd,bknd->bngqk", grouped, block_keys, preferred_element_type=jnp.float32
    ) * HEAD_DIM ** (-0.5)
    scores = jnp.where(live[:, None, None], scores, -jnp.inf)
    highest = jnp.max(scores, axis=-1, keepdims=True)
    weights = jnp.exp(scores - highest)
    total = jnp.sum(weights, axis=-1)
    summed = jnp.einsum(
        "bngqk,bknd->bqngd",
        weights.astype(jnp.bfloat16),
        block_values,
        preferred_element_type=jnp.float32,
    )
    result = summed / jnp.transpose(total, (0, 3, 1, 2))[..., None]
    attended = result.astype(jnp.bfloat16).reshape(rows, heads_dev * HEAD_DIM)
    whole = lax.all_gather(attended, "tp", axis=1, tiled=True)
    mixed = jnp.dot(whole, w_out, preferred_element_type=jnp.float32).astype(jnp.bfloat16)
    return mixed[None]


def solution(mesh):
    placed = (P("dp", "kv", None), P("dp", None), P("dp", "kv", None), P(None, "tp"), P(), P(), P())
    return jax.shard_map(
        shards, mesh=mesh, in_specs=placed, out_specs=P("dp", "kv", None), check_vma=False
    )
```

profile of v0, /device:TPU:0, one launch (start us, length us, event | category | flops | bytes accessed | tf_op | source)
XLA Modules:
  0.0 83.3 jit_solution(2517462831864149929)
XLA Ops:
  0.0 0.0 copy-start
  0.0 0.9 %reduce-window.8 = s32[8,1]{0,1:T(1,128)S(1)} reduce-window(s32[8,1]{0,1:T(1,128)} %bitcast.114, s32[]{:T(128)} %constant.13.clone.1), window={size=8x1 pad=7_0x0_0}, to_apply=%region_0.0 | reduce-window | flops 56 | bytes 68 | tf_op jit(solution)/shard_map/reduce-window.3
  0.9 0.7 broadcast_compare_fusion
  1.6 0.7 maximum_multiply_fusion
  2.3 0.1 convert_reduce_fusion.1
  2.4 0.1 add.96
  2.5 0.1 broadcast_in_dim.12
  2.6 0.1 and.23
  2.7 0.0 copy-done
  2.7 1.7 %fusion.15 = bf16[192,64]{0,1:T(8,128)(2,1)S(1)} fusion(bf16[1,192,2048]{2,1,0:T(8,128)(2,1)S(1)} %copy-done, bf16[2048,128]{1,0:T(8,128)(2,1)} %param.12, s32[]{:T(128)S(6)} %select_n.18), kind=kOutput, calls=%fused_computation.20 | convolution fusion | flops 50343936 | bytes 1335300 | tf_op jit(solution)/shard_map/dot_general | solution.py:53
  4.4 1.6 %convolution_bitcast_fusion = f32[192,1,64]{0,2,1:T(8,128)S(1)} fusion(bf16[1,192,2048]{2,1,0:T(8,128)(2,1)S(1)} %copy-done, bf16[2048,128]{1,0:T(8,128)(2,1)} %param.11, s32[]{:T(128)S(6)} %select_n.18), kind=kOutput, calls=%fused_computation.18 | convolution fusion | flops 50331648 | bytes 1359876 | tf_op jit(solution)/shard_map/dot_general | solution.py:48
  6.1 0.2 fusion.40
  6.3 0.1 copy.26
  6.4 0.8 multiply_cosine_fusion
  7.3 0.1 add.93
  7.3 0.1 add.101
  7.4 0.1 add.94
  7.6 0.1 convert_reduce_fusion
  7.7 0.4 compare_and_fusion
  8.1 32.8 %all_gather.6 = bf16[1536,128]{1,0:T(8,128)(2,1)S(1)} all-gather(bf16[192,128]{1,0:T(8,128)(2,1)S(1)} %copy.26), channel_id=1, replica_groups=mesh['dp'=2,'kv'=8,'tp'=2] {'kv'}, dimensions={0}, use_global_device_ids=true | all-gather | bytes 442368 | tf_op jit(solution)/shard_map/all_gather | solution.py:63
  40.9 0.0 copy-start.1
  40.9 22.0 %gather_fusion = bf16[6144,128]{1,0:T(8,128)(2,1)} fusion(bf16[1536,128]{1,0:T(8,128)(2,1)S(1)} %all_gather.6, s32[6144]{0:T(1024)S(1)} %broadcast_clamp_fusion), kind=kCustom, calls=%fused_computation | custom fusion | bytes 3170304 | tf_op jit(solution)/shard_map/gather | solution.py:64
  62.9 0.0 copy-start.3
  62.9 0.0 copy-done.1
  62.9 2.5 %copy.29 = bf16[2048,512]{0,1:T(8,128)(2,1)} copy(bf16[2048,512]{1,0:T(8,128)(2,1)S(1)} %copy-done.1) | data formatting | bytes 4194304 | tf_op args[3]
  65.4 0.0 copy-start.2
  65.4 2.4 %fusion.22 = f32[192,8,64]{0,2,1:T(8,128)S(1)} fusion(bf16[8,64,2048]{2,1,0:T(8,128)(2,1)} %bitcast.106, bf16[1,192,2048]{2,1,0:T(8,128)(2,1)S(1)} %copy-done), kind=kOutput, calls=%fused_computation.23 | convolution fusion | flops 402653184 | bytes 3276800 | tf_op jit(solution)/shard_map/dot_general | solution.py:40
  67.8 0.0 copy-done.3
  67.9 0.1 subtract_convert_fusion
  67.9 0.3 concatenate.26
  68.2 1.1 %copy.30 = bf16[6,32,8,32]{3,1,2,0:T(8,128)(2,1)} copy(bf16[6,32,8,32]{1,0,3,2:T(8,128)(2,1)S(1)} %concatenate.26) | data formatting | bytes 196608 | tf_op jit(solution)/shard_map/concatenate | solution.py:20
  69.3 0.3 concatenate.27
  69.5 1.1 %copy.31 = bf16[6,32,8,32]{3,1,2,0:T(8,128)(2,1)} copy(bf16[6,32,8,32]{1,0,3,2:T(8,128)(2,1)S(1)} %concatenate.27) | data formatting | bytes 196608 | tf_op jit(solution)/shard_map/concatenate | solution.py:20
  70.6 0.0 copy-done.2
  70.6 2.3 %fusion.2 = (f32[6,8,32]{2,1,0:T(8,128)S(1)}, f32[6,1024,32,8]{1,2,3,0:T(8,128)S(1)}) fusion(pred[6,32,1024]{2,1,0:T(8,128)(4,1)S(1)} %compare_and_fusion, bf16[6,32,8,32]{3,1,2,0:T(8,128)(2,1)} %copy.31, bf16[6,32,8,32]{3,1,2,0:T(8,128)(2,1)} %copy.30, bf16[6,1024,128]{2,1,0:T(8,128)(2,1)S(1)} %bitcast.107), kind=kOutput, calls=%fused_computation.5 | convolution fusion | flops 206436864 | bytes 8263680 | tf_op jit(solution)/shard_map/bqngd,bknd->bngqk/dot_general | solution.py:75
  72.9 1.6 %fusion = f32[6,8,32]{2,1,0:T(8,128)S(1)} fusion(f32[6,1024,32,8]{1,2,3,0:T(8,128)S(1)} %get-tuple-element.12, f32[6,8,32]{2,1,0:T(8,128)S(1)} %get-tuple-element.11, pred[6,32,1024]{2,1,0:T(8,128)(4,1)S(1)} %compare_and_fusion), kind=kLoop, calls=%fused_computation.3 | loop fusion | flops 6289920 | bytes 6500352 | tf_op jit(solution)/shard_map/reduce_sum | solution.py:81
  74.6 2.1 %fusion.19 = bf16[6,32,1,8,64]{4,1,3,0,2:T(8,128)(2,1)S(1)} fusion(f32[6,1024,32,8]{1,2,3,0:T(8,128)S(1)} %get-tuple-element.12, f32[6,8,32]{2,1,0:T(8,128)S(1)} %get-tuple-element.11, pred[6,32,1024]{2,1,0:T(8,128)(4,1)S(1)} %compare_and_fusion, bf16[6,1024,128]{2,1,0:T(8,128)(2,1)S(1)} %bitcast.108, f32[6,32,8]{1,2,0:T(8,128)S(1)} %bitcast.109), kind=kOutput, calls=%fused_computation.22 | convolution fusion | flops 207814656 | bytes 8269824 | tf_op jit(solution)/shard_map/bngqk,bknd->bqngd/dot_general | solution.py:82
  76.7 0.2 copy.32
  76.9 0.3 reshape.293
  77.1 2.1 %all_gather.7 = bf16[192,1024]{1,0:T(8,128)(2,1)S(1)} all-gather(bf16[192,512]{1,0:T(8,128)(2,1)S(1)} %reshape.293), channel_id=1, replica_groups=mesh['dp'=2,'kv'=8,'tp'=2] {'tp'}, dimensions={1}, use_global_device_ids=true | all-gather | bytes 589824 | tf_op jit(solution)/shard_map/all_gather | solution.py:90
  79.2 4.1 %fusion.10 = bf16[1,192,2048]{2,1,0:T(8,128)(2,1)} fusion(bf16[192,1024]{1,0:T(8,128)(2,1)S(1)} %all_gather.7, bf16[1024,2048]{1,0:T(8,128)(2,1)} %param.13), kind=kOutput, calls=%fused_computation.13 | convolution fusion | flops 805699584 | bytes 5373952 | tf_op jit(solution)/shard_map/dot_general | solution.py:91
  (11 shorter events, 0.1 us)
Async XLA Ops:
  0.0 2.7 %copy-start = (bf16[1,192,2048]{2,1,0:T(8,128)(2,1)S(1)}, bf16[1,192,2048]{2,1,0:T(8,128)(2,1)}, u32[]{:S(2)}) copy-start(bf16[1,192,2048]{2,1,0:T(8,128)(2,1)} %param.7) | copy-start | bytes 2359300
  40.9 22.0 %copy-start.1 = (bf16[2048,512]{1,0:T(8,128)(2,1)S(1)}, bf16[2048,512]{1,0:T(8,128)(2,1)}, u32[]{:S(2)}) copy-start(bf16[2048,512]{1,0:T(8,128)(2,1)} %param.10) | copy-start | bytes 6291460
  62.9 4.9 %copy-start.3 = (f32[192,32]{0,1:T(8,128)S(1)}, f32[192,32]{0,1:T(8,128)}, u32[]{:S(2)}) copy-start(f32[192,32]{0,1:T(8,128)} %get-tuple-element.10) | copy-start | bytes 73732
  65.4 5.2 %copy-start.2 = (bf16[6144,128]{1,0:T(8,128)(2,1)S(1)}, bf16[6144,128]{1,0:T(8,128)(2,1)}, u32[]{:S(2)}) copy-start(bf16[6144,128]{1,0:T(8,128)(2,1)} %gather_fusion) | copy-start | bytes 4718596
where the time goes:
time: 83.7 us; the launch traced here: 83.3 us
  blocking collectives  34.9 us (42%)
  local copies, waits for them, and re-layouts  28.3 us (34%)
  matrix products  14.3 us (17%)
  other arithmetic  5.67 us (7%)
    all_gather x1, blocking collectives, shards(): every = lax.all_gather(packed, 'kv', axis=0, tiled=True)  32.8 us
    gather x1, local copies, waits for them, and re-layouts, shards(): selected = every[key_pos]  22 us
    dot_general x1, matrix products, shards(): jnp.dot(whole, w_out, preferred_element_type=jnp.float32)  4.07 us
    concatenate x4, local copies, waits for them, and re-layouts, rotate(): jnp.concatenate([first * cosine - second * sine, second * cosine + first...  2.67 us
    unnamed x11, local copies, waits for them, and re-layouts  2.5 us
    dot_general x1, matrix products, shards(): jnp.dot(local, w_query, preferred_element_type=jnp.float32)  2.44 us
    dot_general x1, matrix products, shards(): jnp.einsum('bqngd,bknd->bngqk', grouped, block_keys, preferred_element_ty...  2.3 us
    dot_general x1, matrix products, shards(): jnp.einsum('bngqk,bknd->bqngd', weights.astype(jnp.bfloat16), block_value...  2.13 us

commit v1 on v0

v1 whole, which is shorter than its diff:
```python
import functools

import jax
import jax.numpy as jnp
import numpy as np
from jax import lax
from jax.experimental import pallas as pl
from jax.experimental.pallas import tpu as pltpu
from jax.sharding import PartitionSpec as P

HEAD_DIM = 64
BLOCK = 32
LANES = 128
HOT = 2
MESH = pl.DeviceIdType.MESH
SCALE = float(HEAD_DIM ** -0.5 * np.log2(np.e))
F32 = jnp.float32
BF16 = jnp.bfloat16


def tables(rows, count):
    lane = np.arange(LANES)
    half = HEAD_DIM // 2
    inverse = (10000.0 ** (-(lane % half) / half)).astype(np.float32).astype(np.float64)
    sign = np.where(lane % HEAD_DIM < half, -1.0, 1.0)
    row = np.arange(rows)[:, None] * inverse
    start = (np.arange(count) * rows)[:, None] * inverse
    inner = np.stack([np.cos(row), np.sin(row) * sign]).astype(np.float32)
    outer = np.zeros((count, 8, LANES), np.float32)
    outer[:, 0] = np.cos(start)
    outer[:, 1] = np.sin(start) * sign
    return inner, outer


def iota(shape, axis):
    return lax.broadcasted_iota(jnp.int32, shape, axis)


def dot_t(a, b):
    return lax.dot_general(a, b, (((1,), (1,)), ((), ())), preferred_element_type=F32)


def dot(a, b):
    return jnp.dot(a, b, preferred_element_type=F32)


def kernel(
    n, tok_hbm, doc_hbm, pick_hbm, wq_hbm, wk_hbm, wv_hbm, wo_hbm, inner_hbm, outer_hbm, out_hbm,
    tok, doc, pick, wq, wk, wv, wo, inner, outer, names, names_in, kv_own, pack, hot_in,
    q_all, acc, top, att, att_in, partial, out, load_sem, name_s, name_r, hot_s, hot_r, att_s, att_r, out_sem,
):
    kv = lax.axis_index("kv")
    tp = lax.axis_index("tp")
    rows = tok.shape[0]
    blocks = rows // BLOCK
    heads = wq.shape[1] // HEAD_DIM
    wide = names.shape[1]
    mine = wo.shape[1]

    barrier = pltpu.get_barrier_semaphore()

    def greet(d, _):
        @pl.when(d != kv)
        def _():
            pl.semaphore_signal(barrier, inc=1, device_id={"kv": d}, device_id_type=MESH)
        return 0

    lax.fori_loop(0, n, greet, 0)
    pl.semaphore_signal(barrier, inc=1, device_id={"tp": 1 - tp}, device_id_type=MESH)

    pairs = [
        (pick_hbm.at[0], pick), (doc_hbm, doc), (tok_hbm.at[0], tok), (wk_hbm, wk), (wv_hbm, wv),
        (inner_hbm, inner), (outer_hbm.at[kv], outer), (wq_hbm, wq),
        (wo_hbm.at[pl.ds(tp * mine, mine)], wo.at[0]), (wo_hbm.at[pl.ds((1 - tp) * mine, mine)], wo.at[1]),
    ]
    loads = [pltpu.make_async_copy(a, b, load_sem.at[i]) for i, (a, b) in enumerate(pairs)]
    for load in loads:
        load.start()
    l_pick, l_doc, l_tok, l_wk, l_wv, l_in, l_out, l_wq, l_wo0, l_wo1 = loads

    l_pick.wait()
    slots = pick[...]
    block_ids = iota((blocks, wide), 1)
    hit = slots[:, 0:1] == block_ids
    for s in range(1, slots.shape[1]):
        hit = hit | (slots[:, s:s + 1] == block_ids)
    named_any = jnp.max(jnp.where(hit, 1.0, 0.0), axis=0, keepdims=True)
    names[...] = jnp.broadcast_to(named_any, names.shape)

    pl.semaphore_wait(barrier, n)

    def name_copy(d, source):
        return pltpu.make_async_remote_copy(
            src_ref=names, dst_ref=names_in.at[source], send_sem=name_s.at[d], recv_sem=name_r.at[source],
            device_id={"kv": d}, device_id_type=MESH)

    def name_send(d, _):
        name_copy(d, kv).start()
        return 0

    lax.fori_loop(0, kv, name_send, 0)

    def clear(d, _):
        hot_in[d] = jnp.zeros(hot_in.shape[1:], BF16)
        return 0

    lax.fori_loop(kv, n, clear, 0)

    l_in.wait()
    l_out.wait()
    cos_o, sin_o = outer[0:1, :], outer[1:2, :]
    cos_i, sin_i = inner[0], inner[1]
    cosine = cos_o * cos_i - sin_o * sin_i
    sine = sin_o * cos_i + cos_o * sin_i
    lane = iota((rows, LANES), 1)
    low = lane < HEAD_DIM
    first = lane % HEAD_DIM < HEAD_DIM // 2
    quarter = HEAD_DIM // 2

    def rotate(x):
        other = jnp.where(first, pltpu.roll(x, LANES - quarter, 1), pltpu.roll(x, quarter, 1))
        return x * cosine + other * sine

    def swap(x):
        return pltpu.roll(x, HEAD_DIM, 1)

    l_tok.wait()
    l_wk.wait()
    l_wv.wait()
    keys = rotate(dot(tok[...], wk[...]))
    values = dot(tok[...], wv[...])
    is_first = tp == 0
    keys = jnp.where(is_first, keys, swap(keys))
    values = jnp.where(is_first, swap(values), values)
    packed = jnp.where(low, keys, values).astype(BF16)
    kv_own[...] = packed

    def name_take(d, total):
        name_copy(d, d).wait_recv()
        return total + names_in[d]

    total = lax.fori_loop(kv + 1, n, name_take, jnp.zeros(names.shape, F32))
    flags = jnp.where(total > 0.0, 1.0, 0.0).astype(BF16)
    j = iota((wide, rows), 0) - kv * blocks
    col = iota((wide, rows), 1) // BLOCK
    here = dot(flags, jnp.where(j == col, 1.0, 0.0).astype(BF16))[0:1, :]
    rank = dot(flags, jnp.where((j >= 0) & (j < col), 1.0, 0.0).astype(BF16))[0:1, :]
    kept = HOT * BLOCK
    slot = iota((2 * kept, rows), 0) % kept
    own = iota((2 * kept, rows), 1)
    choose = (here > 0.5) & (rank == (slot // BLOCK).astype(F32)) & (own % BLOCK == slot % BLOCK)
    choose = jnp.where(choose, 1.0, 0.0).astype(BF16)
    label = (iota((16, rows), 1) // BLOCK + 1).astype(F32).astype(BF16)
    pack[0:kept, :] = dot(choose[0:kept], packed).astype(BF16)
    pack[kept:kept + 16, :] = dot_t(label, choose).astype(BF16)

    def hot_copy(d, source):
        return pltpu.make_async_remote_copy(
            src_ref=pack, dst_ref=hot_in.at[source], send_sem=hot_s.at[d], recv_sem=hot_r.at[source],
            device_id={"kv": d}, device_id_type=MESH)

    def hot_send(d, _):
        hot_copy(d, kv).start()
        return 0

    lax.fori_loop(kv + 1, n, hot_send, 0)

    l_wq.wait()
    queries = dot(tok[...], wq[...])
    for p in range(heads // 2):
        turned = rotate(queries[:, p * LANES:(p + 1) * LANES])
        q_all[2 * p * rows:(2 * p + 1) * rows, :] = jnp.where(low, turned, 0.0).astype(BF16)
        q_all[(2 * p + 1) * rows:(2 * p + 2) * rows, :] = jnp.where(low, swap(turned), 0.0).astype(BF16)

    l_doc.wait()
    q_pos = kv * rows + iota((rows, 1), 0)
    q_start = jnp.zeros((rows, 1), jnp.int32)
    end = jnp.int32(0)
    for i in range(doc.shape[1]):
        end = end + doc[0, i]
        q_start = jnp.where(q_pos >= end, end, q_start)

    def bias_of(key_block, key_pos):
        hits = slots[:, 0:1] == key_block
        for s in range(1, slots.shape[1]):
            hits = hits | (slots[:, s:s + 1] == key_block)
        allowed = jnp.where(hits, 0.0, -jnp.inf)
        parts = []
        for b in range(blocks):
            span = slice(b * BLOCK, (b + 1) * BLOCK)
            seen = (key_pos <= q_pos[span]) & (key_pos >= q_start[span])
            parts.append(jnp.where(seen, allowed[b:b + 1, :], -jnp.inf))
        return jnp.concatenate(parts, axis=0)

    def with_ones(block):
        return jnp.where(iota(block.shape, 1) < HEAD_DIM, jnp.ones((), BF16), block)

    local_col = iota((1, rows), 1)
    bias = bias_of(kv * blocks + local_col // BLOCK, kv * rows + local_col)
    both = jnp.concatenate([bias, bias], axis=0)
    ones_values = with_ones(packed)
    for p in range(heads // 2):
        span = slice(2 * p * rows, (2 * p + 2) * rows)
        scores = dot_t(q_all[span, :], packed) * SCALE + both
        highest = jnp.max(scores, axis=-1, keepdims=True)
        weights = jnp.exp2(scores - highest).astype(BF16)
        acc[span, :] = dot(weights, ones_values)
        top[span, :] = jnp.broadcast_to(highest, (2 * rows, LANES))

    def att_copy(h):
        return pltpu.make_async_remote_copy(
            src_ref=att.at[h], dst_ref=att_in.at[h], send_sem=att_s.at[h], recv_sem=att_r.at[h],
            device_id={"tp": 1 - tp}, device_id_type=MESH)

    def hot_wait(d, _):
        hot_copy(d, d).wait_recv()
        return 0

    lax.fori_loop(0, kv, hot_wait, 0)
    near = min(n, 8)
    width = att.shape[2]

    def group(g, last):
        start = g * near
        blocks_in = hot_in[pl.ds(start, near)]
        block = blocks_in[:, 0:kept, :].reshape(near * kept, LANES)
        upper = iota((1, LANES), 1) < kept
        ids = []
        for d in range(0, near, 2):
            even = hot_in[start + d, kept:kept + 16, :][0:1, :].astype(F32).astype(jnp.int32)
            odd = hot_in[start + d + 1, kept:kept + 16, :][0:1, :].astype(F32).astype(jnp.int32)
            even = jnp.where(even > 0, (start + d) * blocks + even - 1, -2)
            odd = jnp.where(odd > 0, (start + d + 1) * blocks + odd - 1, -2)
            ids.append(jnp.where(upper, even, odd))
        key_block = jnp.concatenate(ids, axis=1)
        key_pos = key_block * BLOCK + iota((1, near * kept), 1) % BLOCK
        bias = bias_of(key_block, key_pos)
        both = jnp.concatenate([bias, bias], axis=0)
        ones_values = with_ones(block)
        for p in range(heads // 2):
            span = slice(2 * p * rows, (2 * p + 2) * rows)
            scores = dot_t(q_all[span, :], block) * SCALE + both
            before = top[span, :]
            highest = jnp.maximum(before, jnp.max(scores, axis=-1, keepdims=True))
            weights = jnp.exp2(scores - highest[:, 0:1]).astype(BF16)
            summed = acc[span, :] * jnp.exp2(before - highest) + dot(weights, ones_values)
            if not last:
                acc[span, :] = summed
                top[span, :] = highest
                continue
            even, odd = summed[0:rows], summed[rows:]
            above = jnp.where(low, swap(even), odd)
            below = jnp.where(low, even, swap(odd))
            half, place = divmod(p * LANES, width)
            att[half, :, place:place + LANES] = (above / below).astype(BF16)
            if place + LANES == width:
                att_copy(half).start()

    if n > near:
        def step(g, _):
            group(g, False)
            return 0

        lax.fori_loop(0, n // near - 1, step, 0)
    group(n // near - 1, True)

    l_wo0.wait()
    halves = att.shape[0]
    columns = wo.shape[2]
    piece = columns // 4
    for c in range(4):
        cut = slice(c * piece, (c + 1) * piece)
        value = dot(att[0], wo[0, 0:width, cut])
        for h in range(1, halves):
            value += dot(att[h], wo[0, h * width:(h + 1) * width, cut])
        partial[:, cut] = value
    l_wo1.wait()
    for h in range(halves):
        att_copy(h).wait_recv()
    stores = []
    for c in range(4):
        cut = slice(c * piece, (c + 1) * piece)
        value = partial[:, cut]
        for h in range(halves):
            value += dot(att_in[h], wo[1, h * width:(h + 1) * width, cut])
        out[:, cut] = value.astype(BF16)
        store = pltpu.make_async_copy(out.at[:, cut], out_hbm.at[0, :, cut], out_sem.at[c])
        store.start()
        stores.append(store)
    for store in stores:
        store.wait()

    def name_done(d, _):
        name_copy(d, kv).wait_send()
        return 0

    def hot_done(d, _):
        hot_copy(d, kv).wait_send()
        return 0

    lax.fori_loop(0, kv, name_done, 0)
    lax.fori_loop(kv + 1, n, hot_done, 0)
    for h in range(halves):
        att_copy(h).wait_send()


def solution(mesh):
    n = mesh.shape["kv"]

    def shards(tokens, doc_lengths, picked, w_query, w_key, w_value, w_out):
        _, rows, d = tokens.shape
        blocks = rows // BLOCK
        wide = -(-n * blocks // LANES) * LANES
        q_cols = w_query.shape[1]
        heads = q_cols // HEAD_DIM
        columns = w_out.shape[1]
        inner, outer = tables(rows, n)
        width = q_cols // 2
        dma = pltpu.SemaphoreType.DMA
        payload = HOT * BLOCK + 16
        return pl.pallas_call(
            functools.partial(kernel, n),
            out_shape=jax.ShapeDtypeStruct((1, rows, columns), BF16),
            in_specs=[pl.BlockSpec(memory_space=pl.ANY)] * 9,
            out_specs=pl.BlockSpec(memory_space=pl.ANY),
            scratch_shapes=[
                pltpu.VMEM((rows, d), BF16),
                pltpu.SMEM(doc_lengths.shape, jnp.int32),
                pltpu.VMEM(picked.shape[1:], jnp.int32),
                pltpu.VMEM(w_query.shape, BF16),
                pltpu.VMEM(w_key.shape, BF16),
                pltpu.VMEM(w_value.shape, BF16),
                pltpu.VMEM((2, w_out.shape[0] // 2, columns), BF16),
                pltpu.VMEM(inner.shape, F32),
                pltpu.VMEM(outer.shape[1:], F32),
                pltpu.VMEM((8, wide), F32),
                pltpu.VMEM((n, 8, wide), F32),
                pltpu.VMEM((rows, LANES), BF16),
                pltpu.VMEM((payload, LANES), BF16),
                pltpu.VMEM((n, payload, LANES), BF16),
                pltpu.VMEM((heads * rows, LANES), BF16),
                pltpu.VMEM((heads * rows, LANES), F32),
                pltpu.VMEM((heads * rows, LANES), F32),
                pltpu.VMEM((2, rows, width), BF16),
                pltpu.VMEM((2, rows, width), BF16),
                pltpu.VMEM((rows, columns), F32),
                pltpu.VMEM((rows, columns), BF16),
                dma((10,)), dma((n,)), dma((n,)), dma((n,)), dma((n,)), dma((2,)), dma((2,)), dma((4,)),
            ],
            compiler_params=pltpu.CompilerParams(
                collective_id=0, has_side_effects=True, vmem_limit_bytes=56 * 1024 * 1024
            ),
        )(tokens, doc_lengths, picked, w_query, w_key, w_value, w_out, inner, outer)

    placed = (P("dp", "kv", None), P("dp", None), P("dp", "kv", None), P(None, "tp"), P(), P(), P())
    return jax.shard_map(
        shards, mesh=mesh, in_specs=placed, out_specs=P("dp", "kv", None), check_vma=False
    )
```

time: 83.7 us -> 20.5 us (0.24)
  the two profiles are of different devices: /device:TPU:0 before, /device:TPU:25 now
where the time goes in v1:
time: 20.5 us; the launch traced here: 20.3 us
  Pallas kernels  16.9 us (82%)
  local copies, waits for them, and re-layouts  3.37 us (16%)
    pallas_call x1, Pallas kernels, shards(): pl.pallas_call(functools.partial(kernel, n), out_shape=jax.ShapeDtypeStru...  16.9 us
    unnamed x2, local copies, waits for them, and re-layouts  3.37 us

profile of v1, /device:TPU:25, one launch (start us, length us, event | category | flops | bytes accessed | tf_op | source)
XLA Modules:
  0.0 20.3 jit_solution(9171605330325750084)
XLA Ops:
  0.0 1.3 %copy.10.pick_hbm = s32[1,6,32]{2,1,0:T(8,128)} copy(s32[1,6,32]{2,0,1:T(1,128)} %param.11) | data formatting | bytes 1536 | tf_op args[2]
  1.3 16.9 %shard_map.91 = bf16[1,192,2048]{2,1,0:T(8,128)(2,1)} custom-call(bf16[1,192,2048]{2,1,0:T(8,128)(2,1)} %tok_hbm.1, s32[1,8]{1,0:T(1,128)} %doc_hbm.1, s32[1,6,32]{2,1,0:T(8,128)} %copy.10.pick_hbm, bf16[2048,512]{1,0:T(8,128)(2,1)} %wq_hbm.1, bf16[2048,128]{1,0:T(8,128)(2,1)} %wk_hbm.1, bf16[2048,128]{1,0:T(8,128)(2,1)} %wv_hbm.1, ...), custom_call_target="tpu_custom_call" | custom-call | tf_op jit(solution)/shard_map/pallas_call | solution.py:321
  18.2 2.1 %copy.12 = bf16[1,192,2048]{2,1,0:T(8,128)(2,1)} copy(bf16[1,192,2048]{2,1,0:T(8,128)(2,1)} %shard_map.91) | data formatting | bytes 1572864

commit v2 on v1

--- a/solution.py
+++ b/solution.py
@@ -45,9 +45,9 @@
 
 
 def kernel(
-    n, tok_hbm, doc_hbm, pick_hbm, wq_hbm, wk_hbm, wv_hbm, wo_hbm, inner_hbm, outer_hbm, out_hbm,
-    tok, doc, pick, wq, wk, wv, wo, inner, outer, names, names_in, kv_own, pack, hot_in,
-    q_all, acc, top, att, att_in, partial, out, load_sem, name_s, name_r, hot_s, hot_r, att_s, att_r, out_sem,
+    n, tok_hbm, doc_hbm, pick_hbm, wq_hbm, wk_hbm, wv_hbm, wo_hbm, inner_hbm, outer_hbm, out,
+    tok, doc, pick, wq, wkv, wo, inner, outer, names, names_in, kv_own, pack, hot_in,
+    q_all, acc, top, att, att_in, partial, load_sem, name_s, name_r, hot_s, hot_r, att_s, att_r,
 ):
     kv = lax.axis_index("kv")
     tp = lax.axis_index("tp")
@@ -69,7 +69,7 @@
     pl.semaphore_signal(barrier, inc=1, device_id={"tp": 1 - tp}, device_id_type=MESH)
 
     pairs = [
-        (pick_hbm.at[0], pick), (doc_hbm, doc), (tok_hbm.at[0], tok), (wk_hbm, wk), (wv_hbm, wv),
+        (pick_hbm, pick), (doc_hbm, doc), (tok_hbm.at[0], tok), (wk_hbm, wkv.at[:, 0:LANES]), (wv_hbm, wkv.at[:, LANES:]),
         (inner_hbm, inner), (outer_hbm.at[kv], outer), (wq_hbm, wq),
         (wo_hbm.at[pl.ds(tp * mine, mine)], wo.at[0]), (wo_hbm.at[pl.ds((1 - tp) * mine, mine)], wo.at[1]),
     ]
@@ -79,7 +79,7 @@
     l_pick, l_doc, l_tok, l_wk, l_wv, l_in, l_out, l_wq, l_wo0, l_wo1 = loads
 
     l_pick.wait()
-    slots = pick[...]
+    slots = jnp.concatenate([pick[b] for b in range(blocks)], axis=0)
     block_ids = iota((blocks, wide), 1)
     hit = slots[:, 0:1] == block_ids
     for s in range(1, slots.shape[1]):
@@ -127,8 +127,9 @@
     l_tok.wait()
     l_wk.wait()
     l_wv.wait()
-    keys = rotate(dot(tok[...], wk[...]))
-    values = dot(tok[...], wv[...])
+    both = dot(tok[...], wkv[...])
+    keys = rotate(both[:, 0:LANES])
+    values = both[:, LANES:]
     is_first = tp == 0
     keys = jnp.where(is_first, keys, swap(keys))
     values = jnp.where(is_first, swap(values), values)
@@ -277,18 +278,12 @@
     l_wo1.wait()
     for h in range(halves):
         att_copy(h).wait_recv()
-    stores = []
     for c in range(4):
         cut = slice(c * piece, (c + 1) * piece)
         value = partial[:, cut]
         for h in range(halves):
             value += dot(att_in[h], wo[1, h * width:(h + 1) * width, cut])
-        out[:, cut] = value.astype(BF16)
-        store = pltpu.make_async_copy(out.at[:, cut], out_hbm.at[0, :, cut], out_sem.at[c])
-        store.start()
-        stores.append(store)
-    for store in stores:
-        store.wait()
+        out[0, :, cut] = value.astype(BF16)
 
     def name_done(d, _):
         name_copy(d, kv).wait_send()
@@ -318,18 +313,19 @@
         width = q_cols // 2
         dma = pltpu.SemaphoreType.DMA
         payload = HOT * BLOCK + 16
+        operands = (tokens, doc_lengths, jnp.transpose(picked, (1, 0, 2)), w_query, w_key, w_value, w_out, inner, outer)
+        operands = [pltpu.with_memory_space_constraint(jnp.asarray(x), pltpu.HBM) for x in operands]
         return pl.pallas_call(
             functools.partial(kernel, n),
             out_shape=jax.ShapeDtypeStruct((1, rows, columns), BF16),
-            in_specs=[pl.BlockSpec(memory_space=pl.ANY)] * 9,
-            out_specs=pl.BlockSpec(memory_space=pl.ANY),
+            in_specs=[pl.BlockSpec(memory_space=pltpu.HBM)] * 9,
+            out_specs=pl.BlockSpec(memory_space=pltpu.VMEM),
             scratch_shapes=[
                 pltpu.VMEM((rows, d), BF16),
                 pltpu.SMEM(doc_lengths.shape, jnp.int32),
-                pltpu.VMEM(picked.shape[1:], jnp.int32),
+                pltpu.VMEM((blocks, 1, picked.shape[2]), jnp.int32),
                 pltpu.VMEM(w_query.shape, BF16),
-                pltpu.VMEM(w_key.shape, BF16),
-                pltpu.VMEM(w_value.shape, BF16),
+                pltpu.VMEM((d, 2 * LANES), BF16),
                 pltpu.VMEM((2, w_out.shape[0] // 2, columns), BF16),
                 pltpu.VMEM(inner.shape, F32),
                 pltpu.VMEM(outer.shape[1:], F32),
@@ -344,13 +340,12 @@
                 pltpu.VMEM((2, rows, width), BF16),
                 pltpu.VMEM((2, rows, width), BF16),
                 pltpu.VMEM((rows, columns), F32),
-                pltpu.VMEM((rows, columns), BF16),
-                dma((10,)), dma((n,)), dma((n,)), dma((n,)), dma((n,)), dma((2,)), dma((2,)), dma((4,)),
+                dma((10,)), dma((n,)), dma((n,)), dma((n,)), dma((n,)), dma((2,)), dma((2,)),
             ],
             compiler_params=pltpu.CompilerParams(
-                collective_id=0, has_side_effects=True, vmem_limit_bytes=56 * 1024 * 1024
+                collective_id=0, has_side_effects=True, vmem_limit_bytes=24 * 1024 * 1024
             ),
-        )(tokens, doc_lengths, picked, w_query, w_key, w_value, w_out, inner, outer)
+        )(*operands)
 
     placed = (P("dp", "kv", None), P("dp", None), P("dp", "kv", None), P(None, "tp"), P(), P(), P())
     return jax.shard_map(

time: 20.5 us -> 17.3 us (0.84)
  local copies, waits for them, and re-layouts: 3.37 us -> 0.88 us
  Pallas kernels: 16.9 us -> 16.2 us
    unnamed x2 -> x1, local copies, waits for them, and re-layouts: 3.37 us -> 0.88 us
    pallas_call x1, Pallas kernels: 16.9 us -> 16.2 us  [shards(): pl.pallas_call(functools.partial(kernel, n), out_shape=jax.ShapeDtypeStru...]
where the time goes in v2:
time: 17.3 us; the launch traced here: 17.1 us
  Pallas kernels  16.2 us (94%)
  local copies, waits for them, and re-layouts  0.88 us (5%)
    pallas_call x1, Pallas kernels, shards(): pl.pallas_call(functools.partial(kernel, n), out_shape=jax.ShapeDtypeStru...  16.2 us
    unnamed x1, local copies, waits for them, and re-layouts  0.88 us

profile of v2, /device:TPU:25, one launch (start us, length us, event | category | flops | bytes accessed | tf_op | source)
XLA Modules:
  0.0 17.1 jit_solution(2066094033665566364)
XLA Ops:
  0.0 16.2 %shard_map.91 = bf16[1,192,2048]{2,1,0:T(8,128)(2,1)S(1)} custom-call(bf16[1,192,2048]{2,1,0:T(8,128)(2,1)} %tok_hbm.1, s32[1,8]{1,0:T(1,128)} %doc_hbm.1, s32[6,1,32]{2,1,0:T(1,128)} %bitcast.1, bf16[2048,512]{1,0:T(8,128)(2,1)} %wq_hbm.1, bf16[2048,128]{1,0:T(8,128)(2,1)} %wk_hbm.1, bf16[2048,128]{1,0:T(8,128)(2,1)} %wv_hbm.1, bf16[1024,2048]{1,0:T(8,128)(2,1)} %wo_hbm.1, ...), custom_call_target="tpu_custom_call" | custom-call | tf_op jit(solution)/shard_map/pallas_call | solution.py:318
  16.2 0.9 %copy.11 = bf16[1,192,2048]{2,1,0:T(8,128)(2,1)} copy(bf16[1,192,2048]{2,1,0:T(8,128)(2,1)S(1)} %shard_map.91) | data formatting | bytes 1572864

commit v3 on v2

--- a/solution.py
+++ b/solution.py
@@ -1,4 +1,5 @@
 import functools
+import math
 
 import jax
 import jax.numpy as jnp
@@ -45,9 +46,9 @@
 
 
 def kernel(
-    n, tok_hbm, doc_hbm, pick_hbm, wq_hbm, wk_hbm, wv_hbm, wo_hbm, inner_hbm, outer_hbm, out,
-    tok, doc, pick, wq, wkv, wo, inner, outer, names, names_in, kv_own, pack, hot_in,
-    q_all, acc, top, att, att_in, partial, load_sem, name_s, name_r, hot_s, hot_r, att_s, att_r,
+    n, reach, tok_hbm, doc_hbm, pick_hbm, wq_hbm, wk_hbm, wv_hbm, wo_hbm, inner_hbm, outer_hbm, out,
+    tok, doc, pick, wq, wkv, wo, inner, outer, names, names_in, kv_own, pack, hot_in, ids, ids_in,
+    q_all, acc, top, att, att_in, partial, load_sem, name_s, name_r, hot_s, hot_r, ids_s, ids_r, att_s, att_r,
 ):
     kv = lax.axis_index("kv")
     tp = lax.axis_index("tp")
@@ -59,13 +60,16 @@
 
     barrier = pltpu.get_barrier_semaphore()
 
+    before = jnp.minimum(kv, reach)
+    after = jnp.minimum(n - 1 - kv, reach)
+
     def greet(d, _):
         @pl.when(d != kv)
         def _():
             pl.semaphore_signal(barrier, inc=1, device_id={"kv": d}, device_id_type=MESH)
         return 0
 
-    lax.fori_loop(0, n, greet, 0)
+    lax.fori_loop(kv - before, kv + after + 1, greet, 0)
     pl.semaphore_signal(barrier, inc=1, device_id={"tp": 1 - tp}, device_id_type=MESH)
 
     pairs = [
@@ -87,24 +91,25 @@
     named_any = jnp.max(jnp.where(hit, 1.0, 0.0), axis=0, keepdims=True)
     names[...] = jnp.broadcast_to(named_any, names.shape)
 
-    pl.semaphore_wait(barrier, n)
-
-    def name_copy(d, source):
+    pl.semaphore_wait(barrier, before + after + 1)
+
+    def name_copy(i):
         return pltpu.make_async_remote_copy(
-            src_ref=names, dst_ref=names_in.at[source], send_sem=name_s.at[d], recv_sem=name_r.at[source],
-            device_id={"kv": d}, device_id_type=MESH)
-
-    def name_send(d, _):
-        name_copy(d, kv).start()
-        return 0
-
-    lax.fori_loop(0, kv, name_send, 0)
-
-    def clear(d, _):
-        hot_in[d] = jnp.zeros(hot_in.shape[1:], BF16)
-        return 0
-
-    lax.fori_loop(kv, n, clear, 0)
+            src_ref=names, dst_ref=names_in.at[i], send_sem=name_s.at[i], recv_sem=name_r.at[i],
+            device_id={"kv": kv - 1 - i}, device_id_type=MESH)
+
+    def name_send(i, _):
+        name_copy(i).start()
+        return 0
+
+    lax.fori_loop(0, before, name_send, 0)
+
+    def clear(i, _):
+        hot_in[i] = jnp.zeros(hot_in.shape[1:], BF16)
+        ids_in[i] = jnp.zeros(ids_in.shape[1:], F32)
+        return 0
+
+    lax.fori_loop(before, reach, clear, 0)
 
     l_in.wait()
     l_out.wait()
@@ -136,12 +141,19 @@
     packed = jnp.where(low, keys, values).astype(BF16)
     kv_own[...] = packed
 
-    def name_take(d, total):
-        name_copy(d, d).wait_recv()
-        return total + names_in[d]
-
-    total = lax.fori_loop(kv + 1, n, name_take, jnp.zeros(names.shape, F32))
-    flags = jnp.where(total > 0.0, 1.0, 0.0).astype(BF16)
+    l_wq.wait()
+    queries = dot(tok[...], wq[...])
+    for p in range(heads // 2):
+        turned = rotate(queries[:, p * LANES:(p + 1) * LANES])
+        q_all[2 * p * rows:(2 * p + 1) * rows, :] = jnp.where(low, turned, 0.0).astype(BF16)
+        q_all[(2 * p + 1) * rows:(2 * p + 2) * rows, :] = jnp.where(low, swap(turned), 0.0).astype(BF16)
+
+    def name_take(i, total):
+        name_copy(i).wait_recv()
+        return total + names_in[i]
+
+    total = lax.fori_loop(0, after, name_take, jnp.zeros(names.shape, F32))
+    flags = jnp.broadcast_to(jnp.where(total > 0.0, 1.0, 0.0), (8, wide)).astype(BF16)
     j = iota((wide, rows), 0) - kv * blocks
     col = iota((wide, rows), 1) // BLOCK
     here = dot(flags, jnp.where(j == col, 1.0, 0.0).astype(BF16))[0:1, :]
@@ -152,26 +164,25 @@
     choose = (here > 0.5) & (rank == (slot // BLOCK).astype(F32)) & (own % BLOCK == slot % BLOCK)
     choose = jnp.where(choose, 1.0, 0.0).astype(BF16)
     label = (iota((16, rows), 1) // BLOCK + 1).astype(F32).astype(BF16)
-    pack[0:kept, :] = dot(choose[0:kept], packed).astype(BF16)
-    pack[kept:kept + 16, :] = dot_t(label, choose).astype(BF16)
-
-    def hot_copy(d, source):
+    pack[...] = dot(choose[0:kept], packed).astype(BF16)
+    ids[...] = dot_t(label, choose)[0:1, :]
+
+    def hot_copy(i):
         return pltpu.make_async_remote_copy(
-            src_ref=pack, dst_ref=hot_in.at[source], send_sem=hot_s.at[d], recv_sem=hot_r.at[source],
-            device_id={"kv": d}, device_id_type=MESH)
-
-    def hot_send(d, _):
-        hot_copy(d, kv).start()
-        return 0
-
-    lax.fori_loop(kv + 1, n, hot_send, 0)
-
-    l_wq.wait()
-    queries = dot(tok[...], wq[...])
-    for p in range(heads // 2):
-        turned = rotate(queries[:, p * LANES:(p + 1) * LANES])
-        q_all[2 * p * rows:(2 * p + 1) * rows, :] = jnp.where(low, turned, 0.0).astype(BF16)
-        q_all[(2 * p + 1) * rows:(2 * p + 2) * rows, :] = jnp.where(low, swap(turned), 0.0).astype(BF16)
+            src_ref=pack, dst_ref=hot_in.at[i], send_sem=hot_s.at[i], recv_sem=hot_r.at[i],
+            device_id={"kv": kv + 1 + i}, device_id_type=MESH)
+
+    def ids_copy(i):
+        return pltpu.make_async_remote_copy(
+            src_ref=ids, dst_ref=ids_in.at[i], send_sem=ids_s.at[i], recv_sem=ids_r.at[i],
+            device_id={"kv": kv + 1 + i}, device_id_type=MESH)
+
+    def hot_send(i, _):
+        ids_copy(i).start()
+        hot_copy(i).start()
+        return 0
+
+    lax.fori_loop(0, after, hot_send, 0)
 
     l_doc.wait()
     q_pos = kv * rows + iota((rows, 1), 0)
@@ -213,27 +224,28 @@
             src_ref=att.at[h], dst_ref=att_in.at[h], send_sem=att_s.at[h], recv_sem=att_r.at[h],
             device_id={"tp": 1 - tp}, device_id_type=MESH)
 
-    def hot_wait(d, _):
-        hot_copy(d, d).wait_recv()
-        return 0
-
-    lax.fori_loop(0, kv, hot_wait, 0)
-    near = min(n, 8)
+    def hot_wait(i, _):
+        ids_copy(i).wait_recv()
+        hot_copy(i).wait_recv()
+        return 0
+
+    lax.fori_loop(0, before, hot_wait, 0)
+    near = math.gcd(reach, 8)
     width = att.shape[2]
 
     def group(g, last):
         start = g * near
-        blocks_in = hot_in[pl.ds(start, near)]
-        block = blocks_in[:, 0:kept, :].reshape(near * kept, LANES)
+        block = hot_in[pl.ds(start, near)].reshape(near * kept, LANES)
         upper = iota((1, LANES), 1) < kept
-        ids = []
-        for d in range(0, near, 2):
-            even = hot_in[start + d, kept:kept + 16, :][0:1, :].astype(F32).astype(jnp.int32)
-            odd = hot_in[start + d + 1, kept:kept + 16, :][0:1, :].astype(F32).astype(jnp.int32)
-            even = jnp.where(even > 0, (start + d) * blocks + even - 1, -2)
-            odd = jnp.where(odd > 0, (start + d + 1) * blocks + odd - 1, -2)
-            ids.append(jnp.where(upper, even, odd))
-        key_block = jnp.concatenate(ids, axis=1)
+        found = []
+        for i in range(0, near, 2):
+            base = (kv - 1 - start - i) * blocks - 1
+            even = ids_in[start + i].astype(jnp.int32)
+            odd = ids_in[start + i + 1].astype(jnp.int32)
+            even = jnp.where(even > 0, base + even, -2)
+            odd = jnp.where(odd > 0, base - blocks + odd, -2)
+            found.append(jnp.where(upper, even, odd))
+        key_block = jnp.concatenate(found, axis=1)
         key_pos = key_block * BLOCK + iota((1, near * kept), 1) % BLOCK
         bias = bias_of(key_block, key_pos)
         both = jnp.concatenate([bias, bias], axis=0)
@@ -257,13 +269,13 @@
             if place + LANES == width:
                 att_copy(half).start()
 
-    if n > near:
+    if reach > near:
         def step(g, _):
             group(g, False)
             return 0
 
-        lax.fori_loop(0, n // near - 1, step, 0)
-    group(n // near - 1, True)
+        lax.fori_loop(0, reach // near - 1, step, 0)
+    group(reach // near - 1, True)
 
     l_wo0.wait()
     halves = att.shape[0]
@@ -285,16 +297,17 @@
             value += dot(att_in[h], wo[1, h * width:(h + 1) * width, cut])
         out[0, :, cut] = value.astype(BF16)
 
-    def name_done(d, _):
-        name_copy(d, kv).wait_send()
-        return 0
-
-    def hot_done(d, _):
-        hot_copy(d, kv).wait_send()
-        return 0
-
-    lax.fori_loop(0, kv, name_done, 0)
-    lax.fori_loop(kv + 1, n, hot_done, 0)
+    def name_done(i, _):
+        name_copy(i).wait_send()
+        return 0
+
+    def hot_done(i, _):
+        ids_copy(i).wait_send()
+        hot_copy(i).wait_send()
+        return 0
+
+    lax.fori_loop(0, before, name_done, 0)
+    lax.fori_loop(0, after, hot_done, 0)
     for h in range(halves):
         att_copy(h).wait_send()
 
@@ -312,11 +325,13 @@
         inner, outer = tables(rows, n)
         width = q_cols // 2
         dma = pltpu.SemaphoreType.DMA
-        payload = HOT * BLOCK + 16
+        payload = HOT * BLOCK
+        reach = min(n, (n * rows // 2 + rows - 2) // rows)
+        reach += reach % 2
         operands = (tokens, doc_lengths, jnp.transpose(picked, (1, 0, 2)), w_query, w_key, w_value, w_out, inner, outer)
         operands = [pltpu.with_memory_space_constraint(jnp.asarray(x), pltpu.HBM) for x in operands]
         return pl.pallas_call(
-            functools.partial(kernel, n),
+            functools.partial(kernel, n, reach),
             out_shape=jax.ShapeDtypeStruct((1, rows, columns), BF16),
             in_specs=[pl.BlockSpec(memory_space=pltpu.HBM)] * 9,
             out_specs=pl.BlockSpec(memory_space=pltpu.VMEM),
@@ -329,18 +344,20 @@
                 pltpu.VMEM((2, w_out.shape[0] // 2, columns), BF16),
                 pltpu.VMEM(inner.shape, F32),
                 pltpu.VMEM(outer.shape[1:], F32),
-                pltpu.VMEM((8, wide), F32),
-                pltpu.VMEM((n, 8, wide), F32),
+                pltpu.VMEM((1, wide), F32),
+                pltpu.VMEM((reach, 1, wide), F32),
                 pltpu.VMEM((rows, LANES), BF16),
                 pltpu.VMEM((payload, LANES), BF16),
-                pltpu.VMEM((n, payload, LANES), BF16),
+                pltpu.VMEM((reach, payload, LANES), BF16),
+                pltpu.VMEM((1, LANES), F32),
+                pltpu.VMEM((reach, 1, LANES), F32),
                 pltpu.VMEM((heads * rows, LANES), BF16),
                 pltpu.VMEM((heads * rows, LANES), F32),
                 pltpu.VMEM((heads * rows, LANES), F32),
                 pltpu.VMEM((2, rows, width), BF16),
                 pltpu.VMEM((2, rows, width), BF16),
                 pltpu.VMEM((rows, columns), F32),
-                dma((10,)), dma((n,)), dma((n,)), dma((n,)), dma((n,)), dma((2,)), dma((2,)),
+                dma((10,)), *[dma((reach,))] * 6, dma((2,)), dma((2,)),
             ],
             compiler_params=pltpu.CompilerParams(
                 collective_id=0, has_side_effects=True, vmem_limit_bytes=24 * 1024 * 1024

time: 17.3 us -> 15.7 us (0.908)
  the two profiles are of different devices: /device:TPU:25 before, /device:TPU:17 now
where the time goes in v3:
time: 15.7 us; the launch traced here: 15.5 us
  Pallas kernels  14.6 us (93%)
  local copies, waits for them, and re-layouts  0.88 us (6%)
    pallas_call x1, Pallas kernels, shards(): pl.pallas_call(functools.partial(kernel, n, reach), out_shape=jax.ShapeDt...  14.6 us
    unnamed x1, local copies, waits for them, and re-layouts  0.88 us

profile of v3, /device:TPU:17, one launch (start us, length us, event | category | flops | bytes accessed | tf_op | source)
XLA Modules:
  0.0 15.5 jit_solution(6945570612197262478)
XLA Ops:
  0.0 14.6 %shard_map.91 = bf16[1,192,2048]{2,1,0:T(8,128)(2,1)S(1)} custom-call(bf16[1,192,2048]{2,1,0:T(8,128)(2,1)} %tok_hbm.1, s32[1,8]{1,0:T(1,128)} %doc_hbm.1, s32[6,1,32]{2,1,0:T(1,128)} %bitcast.1, bf16[2048,512]{1,0:T(8,128)(2,1)} %wq_hbm.1, bf16[2048,128]{1,0:T(8,128)(2,1)} %wk_hbm.1, bf16[2048,128]{1,0:T(8,128)(2,1)} %wv_hbm.1, bf16[1024,2048]{1,0:T(8,128)(2,1)} %wo_hbm.1, ...), custom_call_target="tpu_custom_call" | custom-call | tf_op jit(solution)/shard_map/pallas_call | solution.py:333
  14.6 0.9 %copy.11 = bf16[1,192,2048]{2,1,0:T(8,128)(2,1)} copy(bf16[1,192,2048]{2,1,0:T(8,128)(2,1)S(1)} %shard_map.91) | data formatting | bytes 1572864

commit v4 on v3

--- a/solution.py
+++ b/solution.py
@@ -224,18 +224,21 @@
             src_ref=att.at[h], dst_ref=att_in.at[h], send_sem=att_s.at[h], recv_sem=att_r.at[h],
             device_id={"tp": 1 - tp}, device_id_type=MESH)
 
+    def ids_wait(i, _):
+        ids_copy(i).wait_recv()
+        return 0
+
     def hot_wait(i, _):
-        ids_copy(i).wait_recv()
         hot_copy(i).wait_recv()
         return 0
 
-    lax.fori_loop(0, before, hot_wait, 0)
+    senders = before
+    lax.fori_loop(0, senders, ids_wait, 0)
     near = math.gcd(reach, 8)
     width = att.shape[2]
 
     def group(g, last):
         start = g * near
-        block = hot_in[pl.ds(start, near)].reshape(near * kept, LANES)
         upper = iota((1, LANES), 1) < kept
         found = []
         for i in range(0, near, 2):
@@ -249,6 +252,8 @@
         key_pos = key_block * BLOCK + iota((1, near * kept), 1) % BLOCK
         bias = bias_of(key_block, key_pos)
         both = jnp.concatenate([bias, bias], axis=0)
+        lax.fori_loop(start, jnp.clip(senders, start, start + near), hot_wait, 0)
+        block = hot_in[pl.ds(start, near)].reshape(near * kept, LANES)
         ones_values = with_ones(block)
         for p in range(heads // 2):
             span = slice(2 * p * rows, (2 * p + 2) * rows)

time: 15.7 us -> 15.7 us (level)
  no operation moved by 1% of the time
where the time goes in v4:
time: 15.7 us; the launch traced here: 15.5 us
  Pallas kernels  14.6 us (93%)
  local copies, waits for them, and re-layouts  0.88 us (6%)
    pallas_call x1, Pallas kernels, shards(): pl.pallas_call(functools.partial(kernel, n, reach), out_shape=jax.ShapeDt...  14.6 us
    unnamed x1, local copies, waits for them, and re-layouts  0.88 us

profile of v4, /device:TPU:17, one launch (start us, length us, event | category | flops | bytes accessed | tf_op | source)
XLA Modules:
  0.0 15.5 jit_solution(7451797052575140061)
XLA Ops:
  0.0 14.6 %shard_map.91 = bf16[1,192,2048]{2,1,0:T(8,128)(2,1)S(1)} custom-call(bf16[1,192,2048]{2,1,0:T(8,128)(2,1)} %tok_hbm.1, s32[1,8]{1,0:T(1,128)} %doc_hbm.1, s32[6,1,32]{2,1,0:T(1,128)} %bitcast.1, bf16[2048,512]{1,0:T(8,128)(2,1)} %wq_hbm.1, bf16[2048,128]{1,0:T(8,128)(2,1)} %wk_hbm.1, bf16[2048,128]{1,0:T(8,128)(2,1)} %wv_hbm.1, bf16[1024,2048]{1,0:T(8,128)(2,1)} %wo_hbm.1, ...), custom_call_target="tpu_custom_call" | custom-call | tf_op jit(solution)/shard_map/pallas_call | solution.py:338
  14.6 0.9 %copy.11 = bf16[1,192,2048]{2,1,0:T(8,128)(2,1)} copy(bf16[1,192,2048]{2,1,0:T(8,128)(2,1)S(1)} %shard_map.91) | data formatting | bytes 1572864
